TPU v7x, 32 devices: a whole 2x2x4 slice. The times are simulated.
32 devices in a mesh: ep: 4 (over y, x), tp: 8 (over z, core).
Axes of the slice: x: 2, y: 2, z: 4, core: 2. Of those that a mesh axis runs over, the one named last changes fastest.
Arguments:
- queries: bfloat16 [4096, 1024], P('ep', 'tp'), may hold values from -6 to 6
- keys: bfloat16 [4096, 256], P('ep'), may hold values from -6 to 6, as said below
- values: bfloat16 [4096, 256], P('ep'), may hold values from -6 to 6
- slopes: float32 [16], P('tp'), may hold values from 0.002 to 0.08
- sinks: float32 [16], P('tp'), may hold values from 2 to 6
- out_weight: bfloat16 [1024, 2048], P('tp'), may hold values from -0.1875 to 0.1875
- mix_gain: float32 [2048], replicated, may hold values from 0.1 to 1.9
- moe_input: bfloat16 [4096, 2048], P(('ep', 'tp')), may hold values from -6 to 6
- in_gain: float32 [2048], replicated, may hold values from 0.1 to 1.9
- out_gain: float32 [2048], replicated, may hold values from 0.1 to 1.9
- group_router: bfloat16 [2048, 4], replicated, may hold values from -0.125 to 0.125
- expert_router: bfloat16 [2048, 4], replicated, may hold values from -0.125 to 0.125
- routes: int32 [4096, 2], P(('ep', 'tp')), may hold values from 0 to 3, all different within a row; in each aligned block of 128 rows (0 to 127, 128 to 255, ...) at most 96 rows name the same one
- gate_weight: bfloat16 [4, 2048, 1024], P('ep', None, 'tp'), may hold values from -0.125 to 0.125
- up_weight: bfloat16 [4, 2048, 1024], P('ep', None, 'tp'), may hold values from -0.125 to 0.125
- down_weight: bfloat16 [4, 2048, 1024], P('ep', None, 'tp'), may hold values from -0.1875 to 0.1875
Outputs:
- mixer_output: bfloat16 [4096, 2048], P(('ep', 'tp'))
- moe_output: bfloat16 [4096, 2048], P(('ep', 'tp'))
Inputs may be any that keep to these rules, and one draw needn't show every extreme that they name: `keys`: keys share one value range with the queries. `routes`: A token names 2 different experts. Among the rows of one device no expert is named more than 96 times, a bound that some block reaches in every draw.
All inputs are finite; a program needn't handle non-finite values.
Results may differ from a plain program's by a relative error of at most 0.018.
Values may be sent and summed in bfloat16 or wider, within the bound.
No kernel may reach another device: no remote copies, remote signals or barrier semaphores. Data moves between devices by JAX's collectives and lax.ppermute only.
A program may use at most 128 MiB of HBM per device.

v0:
```python
import math
import jax
import jax.numpy as jnp
from jax import lax
from jax.sharding import PartitionSpec as P

HEADS = 16
HD = 64
KV_HEADS = 4
WINDOW = 128
eps = 1e-06


def shifted(block, axis, distance):
    devices = range(lax.axis_size(axis))
    route = [(i - distance, i) for i in devices if i - distance in devices]
    return lax.ppermute(block, axis, route)


def scale_rows(matrix, gain):
    mean_square = jnp.mean(matrix * matrix, axis=-1, keepdims=True)
    return matrix * lax.rsqrt(mean_square + eps) * gain


def per_device(
    queries,
    keys,
    values,
    slopes,
    sinks,
    out_weight,
    mix_gain,
    moe_input,
    in_gain,
    out_gain,
    group_router,
    expert_router,
    routes,
    gate_weight,
    up_weight,
    down_weight,
):
    rows_group = queries.shape[0]
    local_heads = slopes.shape[0]
    per_kv = HEADS // KV_HEADS
    kv_index = lax.axis_index("tp") * local_heads // per_kv
    own_keys = lax.dynamic_slice_in_dim(keys, kv_index * HD, HD, 1)
    own_values = lax.dynamic_slice_in_dim(values, kv_index * HD, HD, 1)
    rim_keys, rim_values = shifted(
        (own_keys[rows_group - WINDOW :], own_values[rows_group - WINDOW :]), "ep", 1
    )
    blocks = rows_group // WINDOW
    key_blocks = own_keys.reshape(blocks, WINDOW, HD)
    value_blocks = own_values.reshape(blocks, WINDOW, HD)
    key_span = jnp.concatenate(
        [jnp.concatenate([rim_keys[None], key_blocks[:-1]], axis=0), key_blocks], axis=1
    )
    value_span = jnp.concatenate(
        [jnp.concatenate([rim_values[None], value_blocks[:-1]], axis=0), value_blocks], axis=1
    )
    query_blocks = queries.reshape(blocks, WINDOW, local_heads, HD)
    scores = jnp.einsum(
        "nqhd,nsd->nhqs", query_blocks, key_span, preferred_element_type=jnp.float32
    ) * (1.0 / math.sqrt(HD))
    query_index = jnp.arange(WINDOW, dtype=jnp.int32)[:, None]
    key_index = jnp.arange(2 * WINDOW, dtype=jnp.int32)[None, :]
    distance = query_index + WINDOW - key_index
    key_position = (
        lax.axis_index("ep") * rows_group
        + jnp.arange(blocks, dtype=jnp.int32)[:, None, None] * WINDOW
        + key_index[None]
        - WINDOW
    )
    valid = ((distance >= 0) & (distance < WINDOW))[None] & (key_position >= 0)
    scores = scores - slopes[None, :, None, None] * distance.astype(jnp.float32)[None, None]
    scores = jnp.where(valid[:, None], scores, -jnp.inf)
    sink = sinks[None, :, None, None]
    top = jnp.maximum(jnp.max(scores, axis=-1, keepdims=True), sink)
    weights = jnp.exp(scores - top)
    denom = jnp.sum(weights, axis=-1, keepdims=True) + jnp.exp(sink - top)
    probs = (weights / denom).astype(jnp.bfloat16)
    attention = jnp.einsum("nhqs,nsd->nqhd", probs, value_span, preferred_element_type=jnp.float32)
    attention = attention.astype(jnp.bfloat16).reshape(rows_group, local_heads * HD)
    own_rows = moe_input.shape[0]
    projected = lax.psum_scatter(
        jnp.dot(attention, out_weight, preferred_element_type=jnp.float32).astype(jnp.bfloat16),
        "tp",
        scatter_dimension=0,
        tiled=True,
    ).astype(jnp.float32)
    mixer_output = scale_rows(projected, mix_gain).astype(jnp.bfloat16)
    normed = scale_rows(moe_input.astype(jnp.float32), in_gain).astype(jnp.bfloat16)
    group_logits = jnp.dot(normed, group_router, preferred_element_type=jnp.float32)
    expert_logits = jnp.dot(normed, expert_router, preferred_element_type=jnp.float32)
    experts = expert_router.shape[1]
    groups = group_router.shape[1]
    per_group = experts // groups
    visits = routes.shape[1]
    expert_match = routes[:, :, None] == jnp.arange(experts, dtype=jnp.int32)[None, None, :]
    picked_logits = jnp.sum(jnp.where(expert_match, expert_logits[:, None, :], 0.0), axis=-1)
    group_prob = jax.nn.softmax(group_logits, axis=-1)
    group_match = (routes // per_group)[:, :, None] == jnp.arange(groups, dtype=jnp.int32)[
        None, None, :
    ]
    picked_group = jnp.sum(jnp.where(group_match, group_prob[:, None, :], 0.0), axis=-1)
    route_weight = picked_group * jax.nn.softmax(picked_logits, axis=-1)
    capacity = max(2, 3 * own_rows * visits // (2 * experts))
    match_int = expert_match.astype(jnp.int32).reshape(own_rows * visits, experts)
    before = jnp.cumsum(match_int, axis=0) - match_int
    slot = jnp.sum(before * match_int, axis=-1)
    position = (routes.reshape(-1) * capacity + slot).reshape(own_rows, visits)
    slot_ids = jnp.arange(experts * capacity, dtype=jnp.int32)
    placement = jnp.any(position[None, :, :] == slot_ids[:, None, None], axis=-1).astype(
        jnp.bfloat16
    )
    outgoing = jnp.dot(placement, normed, preferred_element_type=jnp.float32).astype(jnp.bfloat16)
    local_experts = gate_weight.shape[0]
    outgoing = outgoing.reshape(lax.axis_size("ep"), local_experts, capacity, normed.shape[1])
    arrived = lax.all_to_all(outgoing, "ep", split_axis=0, concat_axis=0, tiled=True)
    gate_piece = lax.all_gather(gate_weight, "tp", axis=2, tiled=True)
    up_piece = lax.all_gather(up_weight, "tp", axis=2, tiled=True)
    down_piece = lax.all_gather(down_weight, "tp", axis=2, tiled=True)
    gate = jnp.einsum("sxcd,xdf->sxcf", arrived, gate_piece, preferred_element_type=jnp.float32)
    up = jnp.einsum("sxcd,xdf->sxcf", arrived, up_piece, preferred_element_type=jnp.float32)
    hidden = (jax.nn.silu(gate) * up).astype(jnp.bfloat16)
    results = jnp.einsum("sxcf,xdf->sxcd", hidden, down_piece, preferred_element_type=jnp.float32)
    returned = lax.all_to_all(
        results.astype(jnp.bfloat16), "ep", split_axis=0, concat_axis=0, tiled=True
    )
    flat_back = returned.reshape(experts * capacity, returned.shape[3])
    picked_rows = jnp.take(flat_back, position.reshape(-1), axis=0).reshape(
        own_rows, visits, flat_back.shape[1]
    )
    moe = jnp.sum(route_weight[:, :, None] * picked_rows.astype(jnp.float32), axis=1)
    moe_output = scale_rows(moe, out_gain).astype(jnp.bfloat16)
    return (mixer_output, moe_output)


def solution(mesh):
    return jax.shard_map(
        per_device,
        mesh=mesh,
        in_specs=(
            P("ep", "tp"),
            P("ep", None),
            P("ep", None),
            P("tp"),
            P("tp"),
            P("tp", None),
            P(),
            P(("ep", "tp"), None),
            P(),
            P(),
            P(),
            P(),
            P(("ep", "tp"), None),
            P("ep", None, "tp"),
            P("ep", None, "tp"),
            P("ep", None, "tp"),
        ),
        out_specs=(P(("ep", "tp"), None), P(("ep", "tp"), None)),
        check_vma=False,
    )
```

profile of v0, /device:TPU:0, one launch (start us, length us, event | category | flops | bytes accessed | tf_op | source)
XLA Modules:
  0.0 222.8 jit_solution(3067624268574023449)
XLA Ops:
  7.2 0.7 all-gather.6.cloned.1.call-update
  8.0 0.7 all-gather.4.cloned.1.call-update
  8.7 0.7 all-gather.8.cloned.1.call-update
  9.5 1.2 constant_dynamic-slice_fusion
  10.7 0.1 copy.112
  10.9 4.9 %collective-permute-start.1 = (bf16[128,64]{0,1:T(8,128)(2,1)S(1)}, bf16[128,64]{0,1:T(8,128)(2,1)S(1)}, u32[]{:S(2)}, u32[]{:S(2)}) collective-permute-start(bf16[128,64]{0,1:T(8,128)(2,1)S(1)} %slice.36), channel_id=1, source_target_pairs={{0,8},{8,16},{16,24},{1,9},{9,17},{17,25},{2,10},{10,18},{18,26},{... | collective-permute-start | bytes 49160 | tf_op jit(solution)/shard_map/ppermute | solution.py:17
  15.8 0.1 copy.111
  15.9 3.4 %collective-permute-start = (bf16[128,64]{0,1:T(8,128)(2,1)S(1)}, bf16[128,64]{0,1:T(8,128)(2,1)S(1)}, u32[]{:S(2)}, u32[]{:S(2)}) collective-permute-start(bf16[128,64]{0,1:T(8,128)(2,1)S(1)} %slice.34), channel_id=1, source_target_pairs={{0,8},{8,16},{16,24},{1,9},{9,17},{17,25},{2,10},{10,18},{18,26},{... | collective-permute-start | bytes 49160 | tf_op jit(solution)/shard_map/ppermute | solution.py:17
  19.6 0.3 broadcast_and_fusion
  19.9 0.1 broadcast_multiply_fusion
  20.1 0.2 reshape.313
  20.3 0.6 fusion.73
  21.1 0.3 fusion.13
  21.5 0.5 fusion.20
  22.0 0.2 copy.95
  22.2 3.2 %convolution_convert_fusion = bf16[1024,2048]{1,0:T(8,128)(2,1)} fusion(bf16[128,2048]{1,0:T(8,128)(2,1)S(1)} %copy-done, bf16[16,8,8,128]{3,2,1,0:T(8,128)(2,1)S(1)} %bitcast.155), kind=kOutput, calls=%fused_computation.7 | convolution fusion | flops 538968064 | bytes 4980736 | tf_op jit(solution)/shard_map/dot_general | solution.py:86
  25.4 0.6 copy-done.3
  26.1 0.1 copy.97
  26.2 0.1 eq.56
  26.3 0.1 reshape.291
  26.5 1.2 reduce-window.6
  27.8 0.1 copy.99
  27.9 0.1 copy.100
  28.1 0.1 reduce_sum.102
  28.4 0.2 fusion.33
  28.6 1.8 convolution_convert_fusion.1
  30.4 3.9 %all-to-all-start = ((bf16[4,1,96,2048]{3,2,1,0:T(8,128)(2,1)}), bf16[4,1,96,2048]{3,2,1,0:T(8,128)(2,1)S(1)}, u32[]{:S(2)}, u32[]{:S(2)}) async-start(bf16[4,1,96,2048]{3,2,1,0:T(8,128)(2,1)} %bitcast.11), calls=%async_computation.1 | async-start | bytes 3145728 | tf_op jit(solution)/shard_map/all_to_all | solution.py:119
  34.3 0.3 fusion.74
  34.7 0.3 fusion.68
  35.1 0.1 copy.96
  35.2 0.1 copy.105
  35.3 0.1 mul.175
  35.5 17.6 %all-to-all-done = bf16[4,1,96,2048]{3,2,1,0:T(8,128)(2,1)S(1)} async-done(((bf16[4,1,96,2048]{3,2,1,0:T(8,128)(2,1)}), bf16[4,1,96,2048]{3,2,1,0:T(8,128)(2,1)S(1)}, u32[]{:S(2)}, u32[]{:S(2)}) %all-to-all-start) | async-done | bytes 1572896 | tf_op jit(solution)/shard_map/all_to_all | solution.py:119
  53.1 7.1 %all-gather.6.cloned.1.call-done = bf16[1,2048,1024]{2,1,0:T(8,128)(2,1)} async-done(((bf16[1,2048,128]{2,1,0:T(8,128)(2,1)}), bf16[1,2048,1024]{2,1,0:T(8,128)(2,1)}) %all-gather.6.cloned.1.call-update) | async-done | bytes 4194320 | tf_op jit(solution)/shard_map/all_gather | solution.py:121
  60.2 5.1 %fusion.2 = f32[4,96,1024]{2,1,0:T(8,128)} fusion(bf16[1,2048,1024]{2,1,0:T(8,128)(2,1)} %all-gather.6.cloned.1.call-done, bf16[4,1,96,2048]{3,2,1,0:T(8,128)(2,1)S(1)} %all-to-all-done), kind=kOutput, calls=%fused_computation.3 | convolution fusion | flops 1610612736 | bytes 7340032 | tf_op jit(solution)/shard_map/sxcd,xdf->sxcf/dot_general | solution.py:124
  65.3 42.5 %all-gather.4.cloned.1.call-done = bf16[1,2048,1024]{2,1,0:T(8,128)(2,1)} async-done(((bf16[1,2048,128]{2,1,0:T(8,128)(2,1)}), bf16[1,2048,1024]{2,1,0:T(8,128)(2,1)}) %all-gather.4.cloned.1.call-update) | async-done | bytes 4194320 | tf_op jit(solution)/shard_map/all_gather | solution.py:120
  107.8 47.6 %all-gather.8.cloned.1.call-done = bf16[1,2048,1024]{2,1,0:T(8,128)(2,1)} async-done(((bf16[1,2048,128]{2,1,0:T(8,128)(2,1)}), bf16[1,2048,1024]{2,1,0:T(8,128)(2,1)}) %all-gather.8.cloned.1.call-update) | async-done | bytes 4194320 | tf_op jit(solution)/shard_map/all_gather | solution.py:122
  155.4 8.6 %fusion.9 = bf16[4,1,96,2048]{3,2,1,0:T(8,128)(2,1)} fusion(bf16[1,2048,1024]{2,1,0:T(8,128)(2,1)} %all-gather.8.cloned.1.call-done, f32[4,96,1024]{2,1,0:T(8,128)} %fusion.2, bf16[1,2048,1024]{2,1,0:T(8,128)(2,1)} %all-gather.4.cloned.1.call-done, bf16[4,1,96,2048]{3,2,1,0:T(8,128)(2,1)S(1)} %all-to-all-done), kind=kOutput, calls=%fused_computation.10 | convolution fusion | flops 3224371200 | bytes 13107200 | tf_op jit(solution)/shard_map/sxcf,xdf->sxcd/dot_general | solution.py:126
  164.1 3.9 %all-to-all-start.1 = ((bf16[4,1,96,2048]{3,2,1,0:T(8,128)(2,1)}), bf16[4,1,96,2048]{3,2,1,0:T(8,128)(2,1)S(1)}, u32[]{:S(2)}, u32[]{:S(2)}) async-start(bf16[4,1,96,2048]{3,2,1,0:T(8,128)(2,1)} %fusion.9), calls=%async_computation.2 | async-start | bytes 3145728 | tf_op jit(solution)/shard_map/all_to_all | solution.py:127
  167.9 0.1 copy.102
  168.1 37.6 %reduce-scatter.2.cloned.1.call-done = bf16[128,2048]{1,0:T(8,128)(2,1)} async-done(((bf16[1024,2048]{1,0:T(8,128)(2,1)}), bf16[128,2048]{1,0:T(8,128)(2,1)}) %reduce-scatter.2.cloned.1.call-update) | async-done | bytes 524304 | tf_op jit(solution)/shard_map/reduce_scatter | solution.py:85
  205.7 1.2 fusion.30
  207.0 2.0 fusion.32
  209.0 1.4 gather_fusion
  210.4 0.7 gather.7
  211.1 4.1 %multiply_reduce_fusion = f32[128,2048]{1,0:T(8,128)S(1)} fusion(bf16[128,2,2048]{2,1,0:T(2,128)(2,1)S(1)} %gather.7, pred[128,2]{1,0:T(8,128)(4,1)S(1)} %copy.102, f32[128,2]{1,0:T(8,128)S(1)} %copy.96), kind=kLoop, calls=%fused_computation.13 | loop fusion | flops 1835008 | bytes 2098432 | tf_op jit(solution)/shard_map/reduce_sum | solution.py:134
  215.2 0.2 multiply_reduce_fusion.1
  215.3 1.0 multiply_convert_fusion
  (63 shorter events, 1.2 us)
Async XLA Ops:
  7.2 15.0 %copy-start = (bf16[128,2048]{1,0:T(8,128)(2,1)S(1)}, bf16[128,2048]{1,0:T(8,128)(2,1)}, u32[]{:S(2)}) copy-start(bf16[128,2048]{1,0:T(8,128)(2,1)} %param.21) | copy-start | bytes 1572868
  7.2 53.0 %all-gather.6.cloned.1.call-start = ((), (), s32[]{:S(2)}) async-start(), calls=%async_computation.5 | async-start | bytes 4718592 | tf_op jit(solution)/shard_map/all_gather | solution.py:121
  7.9 12.0 %copy-start.8 = (f32[2]{0:T(128)S(1)}, f32[2]{0:T(128)}, u32[]{:S(2)}) copy-start(f32[2]{0:T(128)} %param.19) | copy-start | bytes 28
  7.9 99.9 %all-gather.4.cloned.1.call-start = ((), (), s32[]{:S(2)}) async-start(), calls=%async_computation.4 | async-start | bytes 4718592 | tf_op jit(solution)/shard_map/all_gather | solution.py:120
  8.7 11.4 %copy-start.2 = (bf16[1024,128]{1,0:T(8,128)(2,1)S(1)}, bf16[1024,128]{1,0:T(8,128)(2,1)}, u32[]{:S(2)}) copy-start(bf16[1024,128]{1,0:T(8,128)(2,1)} %param.16) | copy-start | bytes 786436
  8.7 146.7 %all-gather.8.cloned.1.call-start = ((), (), s32[]{:S(2)}) async-start(), calls=%async_computation.6 | async-start | bytes 4718592 | tf_op jit(solution)/shard_map/all_gather | solution.py:122
  9.4 196.3 %reduce-scatter.2.cloned.1.call-start = ((), (), s32[]{:S(2)}) async-start(), calls=%async_computation.3 | async-start | bytes 4718592 | tf_op jit(solution)/shard_map/reduce_scatter | solution.py:85
  10.9 9.4 %collective-permute-start.1 = (bf16[128,64]{0,1:T(8,128)(2,1)S(1)}, bf16[128,64]{0,1:T(8,128)(2,1)S(1)}, u32[]{:S(2)}, u32[]{:S(2)}) collective-permute-start(bf16[128,64]{0,1:T(8,128)(2,1)S(1)} %slice.36), channel_id=1, source_target_pairs={{0,8},{8,16},{16,24},{1,9},{9,17},{17,25},{2,10},{10,18},{18,26},{... | collective-permute-start | bytes 49160 | tf_op jit(solution)/shard_map/ppermute | solution.py:17
  15.9 5.6 %collective-permute-start = (bf16[128,64]{0,1:T(8,128)(2,1)S(1)}, bf16[128,64]{0,1:T(8,128)(2,1)S(1)}, u32[]{:S(2)}, u32[]{:S(2)}) collective-permute-start(bf16[128,64]{0,1:T(8,128)(2,1)S(1)} %slice.34), channel_id=1, source_target_pairs={{0,8},{8,16},{16,24},{1,9},{9,17},{17,25},{2,10},{10,18},{18,26},{... | collective-permute-start | bytes 49160 | tf_op jit(solution)/shard_map/ppermute | solution.py:17
  20.3 0.7 copy-start.7
  25.4 0.7 copy-start.3
  25.4 3.0 %copy-start.1 = (bf16[128,2048]{1,0:T(8,128)(2,1)S(1)}, bf16[128,2048]{1,0:T(8,128)(2,1)}, u32[]{:S(2)}) copy-start(bf16[128,2048]{1,0:T(8,128)(2,1)} %param.23) | copy-start | bytes 1572868
  25.4 3.2 %copy-start.4 = (f32[2048]{0:T(1024)S(1)}, f32[2048]{0:T(1024)}, u32[]{:S(2)}) copy-start(f32[2048]{0:T(1024)} %param.24) | copy-start | bytes 24580
  30.4 3.9 %copy-start.9 = (bf16[2048,4]{0,1:T(4,128)(2,1)S(1)}, bf16[2048,4]{0,1:T(4,128)(2,1)}, u32[]{:S(2)}) copy-start(bf16[2048,4]{0,1:T(4,128)(2,1)} %param.26) | copy-start | bytes 49156
  30.4 4.3 %copy-start.10 = (bf16[2048,4]{0,1:T(4,128)(2,1)S(1)}, bf16[2048,4]{0,1:T(4,128)(2,1)}, u32[]{:S(2)}) copy-start(bf16[2048,4]{0,1:T(4,128)(2,1)} %param.27) | copy-start | bytes 49156
  30.4 22.6 %all-to-all-start = ((bf16[4,1,96,2048]{3,2,1,0:T(8,128)(2,1)}), bf16[4,1,96,2048]{3,2,1,0:T(8,128)(2,1)S(1)}, u32[]{:S(2)}, u32[]{:S(2)}) async-start(bf16[4,1,96,2048]{3,2,1,0:T(8,128)(2,1)} %bitcast.11), calls=%async_computation.1 | async-start | bytes 3145728 | tf_op jit(solution)/shard_map/all_to_all | solution.py:119
  164.1 42.9 %copy-start.5 = (f32[2048]{0:T(1024)S(1)}, f32[2048]{0:T(1024)}, u32[]{:S(2)}) copy-start(f32[2048]{0:T(1024)} %param.22) | copy-start | bytes 24580
  164.1 44.9 %all-to-all-start.1 = ((bf16[4,1,96,2048]{3,2,1,0:T(8,128)(2,1)}), bf16[4,1,96,2048]{3,2,1,0:T(8,128)(2,1)S(1)}, u32[]{:S(2)}, u32[]{:S(2)}) async-start(bf16[4,1,96,2048]{3,2,1,0:T(8,128)(2,1)} %fusion.9), calls=%async_computation.2 | async-start | bytes 3145728 | tf_op jit(solution)/shard_map/all_to_all | solution.py:127
  211.1 4.3 %copy-start.6 = (f32[2048]{0:T(1024)S(1)}, f32[2048]{0:T(1024)}, u32[]{:S(2)}) copy-start(f32[2048]{0:T(1024)} %param.25) | copy-start | bytes 24580
Sparse Core Ops, SparseCore 0:
  9.6 50.5 all-gather.5
  61.7 45.9 all-gather.3
  109.4 45.9 all-gather.7
  157.6 48.1 reduce-scatter.1
where the time goes:
time: 223 us
  waiting for transfers between devices  155 us (70%)
  matrix products  20.5 us (9%)
  starting transfers between devices  16.2 us (7%)
  between operations  14.2 us (6%)
  other arithmetic  11.3 us (5%)
  local copies, waits for them, and re-layouts  6.18 us (3%)
    all_gather x1, waiting for transfers between devices, per_device(): down_piece = lax.all_gather(down_weight, 'tp', axis=2, tiled=True)  47.6 us
    all_gather x1, waiting for transfers between devices, per_device(): gate_piece = lax.all_gather(gate_weight, 'tp', axis=2, tiled=True)  42.5 us
    reduce_scatter x1, waiting for transfers between devices, per_device(): lax.psum_scatter(jnp.dot(attention, out_weight, preferred_element_type=jn...  37.6 us
    all_to_all x1, waiting for transfers between devices, per_device(): lax.all_to_all(outgoing, 'ep', split_axis=0, concat_axis=0, tiled=True)  17.6 us
    dot_general x1, matrix products, per_device(): jnp.einsum('sxcf,xdf->sxcd', hidden, down_piece, preferred_element_type=j...  8.63 us
    ppermute x2, starting transfers between devices, shifted(): return lax.ppermute(block, axis, route)  8.27 us
    all_gather x1, waiting for transfers between devices, per_device(): up_piece = lax.all_gather(up_weight, 'tp', axis=2, tiled=True)  7.09 us
    dot_general x1, matrix products, per_device(): jnp.einsum('sxcd,xdf->sxcf', arrived, up_piece, preferred_element_type=jn...  5.13 us
  transfers between devices with their start and end apart: 8, of which 5 were waited for; matrix products, arithmetic and copies ran while one was open for 13% of the time, Pallas kernels for 0%

commit v1 on v0

--- a/solution.py
+++ b/solution.py
@@ -9,6 +9,18 @@
 KV_HEADS = 4
 WINDOW = 128
 eps = 1e-06
+
+
+def product_in_turn(x, axis, dim, contribution):
+    length, index, extent = (lax.axis_size(axis), lax.axis_index(axis), x.shape[dim])
+    right = [(i, (i + 1) % length) for i in range(length)]
+    carried, running = (x, None)
+    for step in range(length):
+        arriving = lax.ppermute(carried, axis, right) if step < length - 1 else None
+        absorb = contribution(carried, (index - step) % length * extent)
+        running = absorb if running is None else running + absorb
+        carried = arriving
+    return running
 
 
 def shifted(block, axis, distance):
@@ -119,11 +131,20 @@
     arrived = lax.all_to_all(outgoing, "ep", split_axis=0, concat_axis=0, tiled=True)
     gate_piece = lax.all_gather(gate_weight, "tp", axis=2, tiled=True)
     up_piece = lax.all_gather(up_weight, "tp", axis=2, tiled=True)
-    down_piece = lax.all_gather(down_weight, "tp", axis=2, tiled=True)
     gate = jnp.einsum("sxcd,xdf->sxcf", arrived, gate_piece, preferred_element_type=jnp.float32)
     up = jnp.einsum("sxcd,xdf->sxcf", arrived, up_piece, preferred_element_type=jnp.float32)
     hidden = (jax.nn.silu(gate) * up).astype(jnp.bfloat16)
-    results = jnp.einsum("sxcf,xdf->sxcd", hidden, down_piece, preferred_element_type=jnp.float32)
+    results = product_in_turn(
+        down_weight,
+        "tp",
+        2,
+        lambda part, at: jnp.einsum(
+            "sxcf,xdf->sxcd",
+            lax.dynamic_slice_in_dim(hidden, at, part.shape[2], axis=3),
+            part,
+            preferred_element_type=jnp.float32,
+        ),
+    )
     returned = lax.all_to_all(
         results.astype(jnp.bfloat16), "ep", split_axis=0, concat_axis=0, tiled=True
     )

time: 223 us -> 203 us (0.910)
  waiting for transfers between devices: 155 us -> 126 us
  matrix products: 20.5 us -> 27.4 us
    ppermute x0 -> x7, waiting for transfers between devices: none -> 99.3 us  [product_in_turn(): arriving = lax.ppermute(carried, axis, right) if step < length - 1 else None]
    all_gather x1 -> x0, waiting for transfers between devices: 47.6 us -> none  [per_device(): down_piece = lax.all_gather(down_weight, 'tp', axis=2, tiled=True)]
    all_gather x1, waiting for transfers between devices: 42.5 us -> 0.01 us  [per_device(): gate_piece = lax.all_gather(gate_weight, 'tp', axis=2, tiled=True)]
    all_to_all x1, waiting for transfers between devices: 17.6 us -> 0.01 us  [per_device(): lax.all_to_all(outgoing, 'ep', split_axis=0, concat_axis=0, tiled=True)]
    reduce_scatter x1, waiting for transfers between devices: 37.6 us -> 25.7 us  [per_device(): lax.psum_scatter(jnp.dot(attention, out_weight, preferred_element_type=jn...]
    all_gather x1, waiting for transfers between devices: 7.09 us -> 0.01 us  [per_device(): up_piece = lax.all_gather(up_weight, 'tp', axis=2, tiled=True)]
    dot_general x1 -> x9, matrix products: 8.63 us -> 15.4 us  [the longest x8 10.8 us: per_device(): jnp.einsum('sxcf,xdf->sxcd', lax.dynamic_slice_in_dim(hidden, at, part.sh...]
  transfers between devices with their start and end apart: 8 -> 14, of which waited for: 5 -> 7; matrix products, arithmetic and copies ran while one was open for 13% -> 18% of each run, Pallas kernels for 0% -> 0%
where the time goes in v1:
time: 203 us; the launch traced here: 202 us
  waiting for transfers between devices  126 us (62%)
  matrix products  27.4 us (13%)
  starting transfers between devices  15.8 us (8%)
  between operations  14.3 us (7%)
  other arithmetic  11.2 us (6%)
  local copies, waits for them, and re-layouts  7.02 us (3%)
    ppermute x7, waiting for transfers between devices, product_in_turn(): arriving = lax.ppermute(carried, axis, right) if step < length - 1 else None  99.3 us
    reduce_scatter x1, waiting for transfers between devices, per_device(): lax.psum_scatter(jnp.dot(attention, out_weight, preferred_element_type=jn...  25.7 us
    dot_general x8, matrix products, per_device(): jnp.einsum('sxcf,xdf->sxcd', lax.dynamic_slice_in_dim(hidden, at, part.sh...  10.8 us
    ppermute x2, starting transfers between devices, shifted(): return lax.ppermute(block, axis, route)  8.27 us
    dot_general x1, matrix products, per_device(): jnp.einsum('sxcd,xdf->sxcf', arrived, up_piece, preferred_element_type=jn...  5.17 us
    dot_general x1, matrix products, per_device(): jnp.einsum('sxcd,xdf->sxcf', arrived, gate_piece, preferred_element_type=...  4.63 us
    reduce_sum x1, other arithmetic, per_device(): jnp.sum(route_weight[:, :, None] * picked_rows.astype(jnp.float32), axis=1)  4.07 us
  transfers between devices with their start and end apart: 14, of which 7 were waited for; matrix products, arithmetic and copies ran while one was open for 18% of the time, Pallas kernels for 0%

profile of v1, /device:TPU:0, one launch (start us, length us, event | category | flops | bytes accessed | tf_op | source)
XLA Modules:
  0.0 202.2 jit_solution(7399285977318363332)
XLA Ops:
  7.2 0.7 all-gather.5.cloned.1.call-update
  8.0 0.7 all-gather.3.cloned.1.call-update
  8.8 1.2 constant_dynamic-slice_fusion
  10.1 4.9 %collective-permute-start.1 = (bf16[128,64]{0,1:T(8,128)(2,1)S(1)}, bf16[128,64]{0,1:T(8,128)(2,1)S(1)}, u32[]{:S(2)}, u32[]{:S(2)}) collective-permute-start(bf16[128,64]{0,1:T(8,128)(2,1)S(1)} %slice.36), channel_id=1, source_target_pairs={{0,8},{8,16},{16,24},{1,9},{9,17},{17,25},{2,10},{10,18},{18,26},{... | collective-permute-start | bytes 49160 | tf_op jit(solution)/shard_map/ppermute | solution.py:29
  15.2 3.4 %collective-permute-start = (bf16[128,64]{0,1:T(8,128)(2,1)S(1)}, bf16[128,64]{0,1:T(8,128)(2,1)S(1)}, u32[]{:S(2)}, u32[]{:S(2)}) collective-permute-start(bf16[128,64]{0,1:T(8,128)(2,1)S(1)} %slice.34), channel_id=1, source_target_pairs={{0,8},{8,16},{16,24},{1,9},{9,17},{17,25},{2,10},{10,18},{18,26},{... | collective-permute-start | bytes 49160 | tf_op jit(solution)/shard_map/ppermute | solution.py:29
  18.9 0.3 broadcast_and_fusion
  19.3 0.2 reshape.390
  19.6 0.6 fusion.94
  20.3 0.3 fusion.6
  20.7 0.5 fusion.13
  21.2 0.2 copy.95
  21.4 3.2 %convolution_convert_fusion = bf16[1024,2048]{1,0:T(8,128)(2,1)} fusion(bf16[128,2048]{1,0:T(8,128)(2,1)S(1)} %copy-done, bf16[16,8,8,128]{3,2,1,0:T(8,128)(2,1)S(1)} %bitcast.183), kind=kOutput, calls=%fused_computation.5 | convolution fusion | flops 538968064 | bytes 4980736 | tf_op jit(solution)/shard_map/dot_general | solution.py:98
  24.7 1.0 copy-done.2
  25.9 0.1 reshape.342
  26.1 21.4 %collective-permute-done.2 = bf16[1,2048,128]{2,1,0:T(8,128)(2,1)S(1)} collective-permute-done((bf16[1,2048,128]{2,1,0:T(8,128)(2,1)S(1)}, bf16[1,2048,128]{2,1,0:T(8,128)(2,1)S(1)}, u32[]{:S(2)}, u32[]{:S(2)}) %collective-permute-start.2) | collective-permute-done | bytes 524320 | tf_op jit(solution)/shard_map/ppermute | solution.py:19
  47.5 1.2 reduce-window.6
  49.1 0.1 reduce_sum.102
  49.3 19.9 %collective-permute-done.3 = bf16[1,2048,128]{2,1,0:T(8,128)(2,1)S(1)} collective-permute-done((bf16[1,2048,128]{2,1,0:T(8,128)(2,1)S(1)}, bf16[1,2048,128]{2,1,0:T(8,128)(2,1)S(1)}, u32[]{:S(2)}, u32[]{:S(2)}) %collective-permute-start.3) | collective-permute-done | bytes 524320 | tf_op jit(solution)/shard_map/ppermute | solution.py:19
  69.2 0.2 fusion.21
  69.4 10.3 %collective-permute-done.4 = bf16[1,2048,128]{2,1,0:T(8,128)(2,1)} collective-permute-done((bf16[1,2048,128]{2,1,0:T(8,128)(2,1)S(1)}, bf16[1,2048,128]{2,1,0:T(8,128)(2,1)}, u32[]{:S(2)}, u32[]{:S(2)}) %collective-permute-start.4) | collective-permute-done | bytes 524320 | tf_op jit(solution)/shard_map/ppermute | solution.py:19
  79.8 1.8 convolution_convert_fusion.1
  81.6 3.7 %all-to-all-start = ((bf16[4,1,96,2048]{3,2,1,0:T(8,128)(2,1)}), bf16[4,1,96,2048]{3,2,1,0:T(8,128)(2,1)S(1)}, u32[]{:S(2)}, u32[]{:S(2)}) async-start(bf16[4,1,96,2048]{3,2,1,0:T(8,128)(2,1)} %bitcast.11), calls=%async_computation.1 | async-start | bytes 3145728 | tf_op jit(solution)/shard_map/all_to_all | solution.py:131
  85.4 0.3 fusion.95
  85.7 15.9 %collective-permute-done.5 = bf16[1,2048,128]{2,1,0:T(8,128)(2,1)} collective-permute-done((bf16[1,2048,128]{2,1,0:T(8,128)(2,1)}, bf16[1,2048,128]{2,1,0:T(8,128)(2,1)}, u32[]{:S(2)}, u32[]{:S(2)}) %collective-permute-start.5) | collective-permute-done | bytes 524320 | tf_op jit(solution)/shard_map/ppermute | solution.py:19
  101.6 0.3 fusion.89
  101.9 21.7 %collective-permute-done.6 = bf16[1,2048,128]{2,1,0:T(8,128)(2,1)} collective-permute-done((bf16[1,2048,128]{2,1,0:T(8,128)(2,1)}, bf16[1,2048,128]{2,1,0:T(8,128)(2,1)}, u32[]{:S(2)}, u32[]{:S(2)}) %collective-permute-start.6) | collective-permute-done | bytes 524320 | tf_op jit(solution)/shard_map/ppermute | solution.py:19
  124.2 10.2 %collective-permute-done.7 = bf16[1,2048,128]{2,1,0:T(8,128)(2,1)S(1)} collective-permute-done((bf16[1,2048,128]{2,1,0:T(8,128)(2,1)}, bf16[1,2048,128]{2,1,0:T(8,128)(2,1)S(1)}, u32[]{:S(2)}, u32[]{:S(2)}) %collective-permute-start.7) | collective-permute-done | bytes 524320 | tf_op jit(solution)/shard_map/ppermute | solution.py:19
  134.3 5.2 %fusion = f32[4,96,1024]{2,1,0:T(8,128)} fusion(bf16[1,2048,1024]{2,1,0:T(8,128)(2,1)} %all-gather.5.cloned.1.call-done, bf16[4,1,96,2048]{3,2,1,0:T(8,128)(2,1)S(1)} %all-to-all-done), kind=kOutput, calls=%fused_computation.1 | convolution fusion | flops 1610612736 | bytes 7340032 | tf_op jit(solution)/shard_map/sxcd,xdf->sxcf/dot_general | solution.py:135
  139.5 4.6 %fusion.7 = bf16[4,1,96,1024]{3,2,0,1:T(8,128)(2,1)S(1)} fusion(f32[4,96,1024]{2,1,0:T(8,128)} %fusion, bf16[1,2048,1024]{2,1,0:T(8,128)(2,1)} %all-gather.3.cloned.1.call-done, bf16[4,1,96,2048]{3,2,1,0:T(8,128)(2,1)S(1)} %all-to-all-done), kind=kOutput, calls=%fused_computation.17 | convolution fusion | flops 1612972032 | bytes 8126464 | tf_op jit(solution)/shard_map/sxcd,xdf->sxcf/dot_general | solution.py:134
  144.2 0.6 fusion.37
  144.7 0.6 fusion.25
  145.3 1.6 fusion.27
  147.0 1.6 fusion.29
  148.6 1.7 fusion.31
  150.3 0.6 fusion.33
  150.9 0.5 copy-done.4
  151.3 0.6 fusion.35
  151.9 3.5 %fusion.4 = bf16[4,1,96,2048]{3,2,1,0:T(8,128)(2,1)} fusion(f32[4,96,2048]{2,1,0:T(8,128)S(1)} %fusion.25, f32[4,96,2048]{2,1,0:T(8,128)S(1)} %fusion.27, f32[4,96,2048]{2,1,0:T(8,128)S(1)} %fusion.29, f32[4,96,2048]{2,1,0:T(8,128)S(1)} %fusion.31, f32[4,96,2048]{2,1,0:T(8,128)S(1)} %fusion.33, f32[4,96,2048]{2,1,0:T(8,128)S(1)} %fusion.37, ...), kind=kOutput, calls=%fused_computation.8 | convolution fusion | flops 207618048 | bytes 24215556 | tf_op jit(solution)/shard_map/sxcf,xdf->sxcd/dot_general | solution.py:141
  155.5 3.7 %all-to-all-start.1 = ((bf16[4,1,96,2048]{3,2,1,0:T(8,128)(2,1)}), bf16[4,1,96,2048]{3,2,1,0:T(8,128)(2,1)S(1)}, u32[]{:S(2)}, u32[]{:S(2)}) async-start(bf16[4,1,96,2048]{3,2,1,0:T(8,128)(2,1)} %fusion.4), calls=%async_computation.2 | async-start | bytes 3145728 | tf_op jit(solution)/shard_map/all_to_all | solution.py:148
  159.2 0.1 copy.102
  159.3 25.7 %reduce-scatter.2.cloned.1.call-done = bf16[128,2048]{1,0:T(8,128)(2,1)} async-done(((bf16[1024,2048]{1,0:T(8,128)(2,1)}), bf16[128,2048]{1,0:T(8,128)(2,1)}) %reduce-scatter.2.cloned.1.call-update) | async-done | bytes 524304 | tf_op jit(solution)/shard_map/reduce_scatter | solution.py:97
  185.1 1.2 fusion.18
  186.3 2.0 %fusion.20 = bf16[128,2048]{1,0:T(8,128)(2,1)} fusion(bf16[128,2048]{1,0:T(8,128)(2,1)} %reduce-scatter.2.cloned.1.call-done, f32[2048]{0:T(1024)S(1)} %copy-done.10, f32[128]{0:T(128)S(1)} %add_rsqrt_fusion.2), kind=kLoop, calls=%fused_computation.33 | loop fusion | flops 1048576 | bytes 1057280 | tf_op jit(solution)/shard_map/convert_element_type | solution.py:103
  188.4 1.4 gather_fusion
  189.7 0.7 gather.7
  190.5 4.1 %multiply_reduce_fusion = f32[128,2048]{1,0:T(8,128)S(1)} fusion(bf16[128,2,2048]{2,1,0:T(2,128)(2,1)S(1)} %gather.7, pred[128,2]{1,0:T(8,128)(4,1)S(1)} %copy.102, f32[128,2]{1,0:T(8,128)S(1)} %copy.96), kind=kLoop, calls=%fused_computation.11 | loop fusion | flops 1835008 | bytes 2098432 | tf_op jit(solution)/shard_map/reduce_sum | solution.py:155
  194.5 0.2 multiply_reduce_fusion.1
  194.7 1.0 multiply_convert_fusion
  (92 shorter events, 2.3 us)
Async XLA Ops:
  7.2 14.3 %copy-start = (bf16[128,2048]{1,0:T(8,128)(2,1)S(1)}, bf16[128,2048]{1,0:T(8,128)(2,1)}, u32[]{:S(2)}) copy-start(bf16[128,2048]{1,0:T(8,128)(2,1)} %param.21) | copy-start | bytes 1572868
  7.2 12.0 %copy-start.13 = (f32[2]{0:T(128)S(1)}, f32[2]{0:T(128)}, u32[]{:S(2)}) copy-start(f32[2]{0:T(128)} %param.19) | copy-start | bytes 28
  7.2 127.2 %all-gather.5.cloned.1.call-start = ((), (), s32[]{:S(2)}) async-start(), calls=%async_computation.5 | async-start | bytes 4718592 | tf_op jit(solution)/shard_map/all_gather | solution.py:133
  7.9 11.4 %copy-start.7 = (bf16[1024,128]{1,0:T(8,128)(2,1)S(1)}, bf16[1024,128]{1,0:T(8,128)(2,1)}, u32[]{:S(2)}) copy-start(bf16[1024,128]{1,0:T(8,128)(2,1)} %param.16) | copy-start | bytes 786436
  7.9 131.6 %all-gather.3.cloned.1.call-start = ((), (), s32[]{:S(2)}) async-start(), calls=%async_computation.4 | async-start | bytes 4718592 | tf_op jit(solution)/shard_map/all_gather | solution.py:132
  8.7 176.4 %reduce-scatter.2.cloned.1.call-start = ((), (), s32[]{:S(2)}) async-start(), calls=%async_computation.3 | async-start | bytes 4718592 | tf_op jit(solution)/shard_map/reduce_scatter | solution.py:97
  10.1 9.4 %collective-permute-start.1 = (bf16[128,64]{0,1:T(8,128)(2,1)S(1)}, bf16[128,64]{0,1:T(8,128)(2,1)S(1)}, u32[]{:S(2)}, u32[]{:S(2)}) collective-permute-start(bf16[128,64]{0,1:T(8,128)(2,1)S(1)} %slice.36), channel_id=1, source_target_pairs={{0,8},{8,16},{16,24},{1,9},{9,17},{17,25},{2,10},{10,18},{18,26},{... | collective-permute-start | bytes 49160 | tf_op jit(solution)/shard_map/ppermute | solution.py:29
  15.2 5.6 %collective-permute-start = (bf16[128,64]{0,1:T(8,128)(2,1)S(1)}, bf16[128,64]{0,1:T(8,128)(2,1)S(1)}, u32[]{:S(2)}, u32[]{:S(2)}) collective-permute-start(bf16[128,64]{0,1:T(8,128)(2,1)S(1)} %slice.34), channel_id=1, source_target_pairs={{0,8},{8,16},{16,24},{1,9},{9,17},{17,25},{2,10},{10,18},{18,26},{... | collective-permute-start | bytes 49160 | tf_op jit(solution)/shard_map/ppermute | solution.py:29
  19.6 0.7 copy-start.12
  24.6 1.0 copy-start.2
  24.6 1.0 copy-start.8
  24.6 44.6 %copy-start.1 = (bf16[128,2048]{1,0:T(8,128)(2,1)S(1)}, bf16[128,2048]{1,0:T(8,128)(2,1)}, u32[]{:S(2)}) copy-start(bf16[128,2048]{1,0:T(8,128)(2,1)} %param.23) | copy-start | bytes 1572868
  24.7 55.1 %copy-start.9 = (f32[2048]{0:T(1024)S(1)}, f32[2048]{0:T(1024)}, u32[]{:S(2)}) copy-start(f32[2048]{0:T(1024)} %param.24) | copy-start | bytes 24580
  25.7 21.8 %collective-permute-start.2 = (bf16[1,2048,128]{2,1,0:T(8,128)(2,1)S(1)}, bf16[1,2048,128]{2,1,0:T(8,128)(2,1)S(1)}, u32[]{:S(2)}, u32[]{:S(2)}) collective-permute-start(bf16[1,2048,128]{2,1,0:T(8,128)(2,1)S(1)} %copy-done.2), channel_id=1, source_target_pairs={{0,1},{1,2},{2,3},{3,4},{4,5},{5,6},{6,7},{7,0},{8,9},{9,10},{10,1... | collective-permute-start | bytes 1572872 | tf_op jit(solution)/shard_map/ppermute | solution.py:19
  47.4 34.2 %copy-start.3 = (bf16[1,2048,128]{2,1,0:T(8,128)(2,1)}, bf16[1,2048,128]{2,1,0:T(8,128)(2,1)S(1)}, u32[]{:S(2)}) copy-start(bf16[1,2048,128]{2,1,0:T(8,128)(2,1)S(1)} %collective-permute-done.2) | copy-start | bytes 1572868
  47.5 21.8 %collective-permute-start.3 = (bf16[1,2048,128]{2,1,0:T(8,128)(2,1)S(1)}, bf16[1,2048,128]{2,1,0:T(8,128)(2,1)S(1)}, u32[]{:S(2)}, u32[]{:S(2)}) collective-permute-start(bf16[1,2048,128]{2,1,0:T(8,128)(2,1)S(1)} %collective-permute-done.2), channel_id=1, source_target_pairs={{0,1},{1,2},{2,3},{3,4},{4,5},{5,6},{6,7},{7,0},{8,9},{9,10},{10,1... | collective-permute-start | bytes 1572872 | tf_op jit(solution)/shard_map/ppermute | solution.py:19
  69.2 12.4 %copy-start.5 = (bf16[1,2048,128]{2,1,0:T(8,128)(2,1)}, bf16[1,2048,128]{2,1,0:T(8,128)(2,1)S(1)}, u32[]{:S(2)}) copy-start(bf16[1,2048,128]{2,1,0:T(8,128)(2,1)S(1)} %collective-permute-done.3) | copy-start | bytes 1572868
  69.2 10.5 %collective-permute-start.4 = (bf16[1,2048,128]{2,1,0:T(8,128)(2,1)S(1)}, bf16[1,2048,128]{2,1,0:T(8,128)(2,1)}, u32[]{:S(2)}, u32[]{:S(2)}) collective-permute-start(bf16[1,2048,128]{2,1,0:T(8,128)(2,1)S(1)} %collective-permute-done.3), channel_id=1, source_target_pairs={{0,1},{1,2},{2,3},{3,4},{4,5},{5,6},{6,7},{7,0},{8,9},{9,10},{10,1... | collective-permute-start | bytes 1572872 | tf_op jit(solution)/shard_map/ppermute | solution.py:19
  79.7 21.8 %collective-permute-start.5 = (bf16[1,2048,128]{2,1,0:T(8,128)(2,1)}, bf16[1,2048,128]{2,1,0:T(8,128)(2,1)}, u32[]{:S(2)}, u32[]{:S(2)}) collective-permute-start(bf16[1,2048,128]{2,1,0:T(8,128)(2,1)} %collective-permute-done.4), channel_id=1, source_target_pairs={{0,1},{1,2},{2,3},{3,4},{4,5},{5,6},{6,7},{7,0},{8,9},{9,10},{10,1... | collective-permute-start | bytes 1572872 | tf_op jit(solution)/shard_map/ppermute | solution.py:19
  81.6 3.7 %copy-start.14 = (bf16[2048,4]{0,1:T(4,128)(2,1)S(1)}, bf16[2048,4]{0,1:T(4,128)(2,1)}, u32[]{:S(2)}) copy-start(bf16[2048,4]{0,1:T(4,128)(2,1)} %param.26) | copy-start | bytes 49156
  81.6 20.0 %copy-start.15 = (bf16[2048,4]{0,1:T(4,128)(2,1)S(1)}, bf16[2048,4]{0,1:T(4,128)(2,1)}, u32[]{:S(2)}) copy-start(bf16[2048,4]{0,1:T(4,128)(2,1)} %param.27) | copy-start | bytes 49156
  81.6 52.7 %all-to-all-start = ((bf16[4,1,96,2048]{3,2,1,0:T(8,128)(2,1)}), bf16[4,1,96,2048]{3,2,1,0:T(8,128)(2,1)S(1)}, u32[]{:S(2)}, u32[]{:S(2)}) async-start(bf16[4,1,96,2048]{3,2,1,0:T(8,128)(2,1)} %bitcast.11), calls=%async_computation.1 | async-start | bytes 3145728 | tf_op jit(solution)/shard_map/all_to_all | solution.py:131
  101.6 22.1 %collective-permute-start.6 = (bf16[1,2048,128]{2,1,0:T(8,128)(2,1)}, bf16[1,2048,128]{2,1,0:T(8,128)(2,1)}, u32[]{:S(2)}, u32[]{:S(2)}) collective-permute-start(bf16[1,2048,128]{2,1,0:T(8,128)(2,1)} %collective-permute-done.5), channel_id=1, source_target_pairs={{0,1},{1,2},{2,3},{3,4},{4,5},{5,6},{6,7},{7,0},{8,9},{9,10},{10,1... | collective-permute-start | bytes 1572872 | tf_op jit(solution)/shard_map/ppermute | solution.py:19
  123.6 10.7 %collective-permute-start.7 = (bf16[1,2048,128]{2,1,0:T(8,128)(2,1)}, bf16[1,2048,128]{2,1,0:T(8,128)(2,1)S(1)}, u32[]{:S(2)}, u32[]{:S(2)}) collective-permute-start(bf16[1,2048,128]{2,1,0:T(8,128)(2,1)} %collective-permute-done.6), channel_id=1, source_target_pairs={{0,1},{1,2},{2,3},{3,4},{4,5},{5,6},{6,7},{7,0},{8,9},{9,10},{10,1... | collective-permute-start | bytes 1572872 | tf_op jit(solution)/shard_map/ppermute | solution.py:19
  134.3 17.6 %collective-permute-start.8 = (bf16[1,2048,128]{2,1,0:T(8,128)(2,1)S(1)}, bf16[1,2048,128]{2,1,0:T(8,128)(2,1)}, u32[]{:S(2)}, u32[]{:S(2)}) collective-permute-start(bf16[1,2048,128]{2,1,0:T(8,128)(2,1)S(1)} %collective-permute-done.7), channel_id=1, source_target_pairs={{0,1},{1,2},{2,3},{3,4},{4,5},{5,6},{6,7},{7,0},{8,9},{9,10},{10,1... | collective-permute-start | bytes 1572872 | tf_op jit(solution)/shard_map/ppermute | solution.py:19
  148.6 1.7 copy-start.6
  150.3 1.1 copy-start.4
  155.5 30.8 %copy-start.10 = (f32[2048]{0:T(1024)S(1)}, f32[2048]{0:T(1024)}, u32[]{:S(2)}) copy-start(f32[2048]{0:T(1024)} %param.22) | copy-start | bytes 24580
  155.5 32.9 %all-to-all-start.1 = ((bf16[4,1,96,2048]{3,2,1,0:T(8,128)(2,1)}), bf16[4,1,96,2048]{3,2,1,0:T(8,128)(2,1)S(1)}, u32[]{:S(2)}, u32[]{:S(2)}) async-start(bf16[4,1,96,2048]{3,2,1,0:T(8,128)(2,1)} %fusion.4), calls=%async_computation.2 | async-start | bytes 3145728 | tf_op jit(solution)/shard_map/all_to_all | solution.py:148
  190.4 4.3 %copy-start.11 = (f32[2048]{0:T(1024)S(1)}, f32[2048]{0:T(1024)}, u32[]{:S(2)}) copy-start(f32[2048]{0:T(1024)} %param.25) | copy-start | bytes 24580
Sparse Core Ops, SparseCore 0:
  9.6 61.7 all-gather.4
  73.0 57.4 all-gather.2
  132.8 52.2 reduce-scatter.1
